TPU v7x, 32 devices: a whole 2x2x4 slice. The times are simulated.
32 devices in a mesh: grp: 2 (over y), kv: 4 (over z), tp: 4 (over x, core).
Axes of the slice: x: 2, y: 2, z: 4, core: 2. Of those that a mesh axis runs over, the one named last changes fastest.
Arguments:
- tokens: bfloat16 [24, 4096], P('grp', ('kv', 'tp')), parts along dimension 0, may hold values from -70 to 70
- attn_gain: bfloat16 [4096], P('kv'), may hold values from 0.099609375 to 1.8984375
- query_weight: bfloat16 [4096, 4096], P('kv', 'tp'), may hold values from -0.09375 to 0.09375
- key_weight: bfloat16 [1024, 4096], P('tp', 'kv'), may hold values from -0.09375 to 0.09375
- value_weight: bfloat16 [1024, 4096], P('tp', 'kv'), may hold values from -0.09375 to 0.09375
- forget_weight: bfloat16 [64, 4096], P(None, 'kv'), may hold values from -0.09375 to 0.09375
- forget_bias: float32 [64], replicated, may hold values from -3 to 1
- cache_keys: bfloat16 [24, 16, 64, 4096], P('grp', 'tp', None, 'kv'), parts along dimension 0, may hold values from -620 to 620
- cache_values: bfloat16 [24, 16, 64, 4096], P('grp', 'tp', None, 'kv'), parts along dimension 0, may hold values from -6 to 6
- gate_sums: float32 [24, 64, 4096], P('grp', 'tp', 'kv'), parts along dimension 0, may hold values from -411.6 to 0
- output_weight: bfloat16 [4096, 4096], P('tp', 'kv'), may hold values from -0.09375 to 0.09375
- mixer_gain: bfloat16 [4096], P('kv'), may hold values from 0.099609375 to 1.8984375
- up_weight: bfloat16 [4096, 16384], P('kv', 'tp'), may hold values from -0.09375 to 0.09375
- down_weight: bfloat16 [16384, 4096], P('tp', 'kv'), may hold values from -0.046875 to 0.046875
Outputs:
- mixed: bfloat16 [24, 4096], P('grp', ('kv', 'tp')), parts along dimension 0
There are 2 independent parts, one for each index of `grp`. A program takes and returns all parts, laid end to end along the dimension named above; an argument that names none is the same for every part. Nothing has to cross between parts.
All inputs are finite; a program needn't handle non-finite values.
Results may differ from a plain program's by a relative error of at most 0.008.
Values may be sent and summed in bfloat16 or wider, within the bound.
A program may use at most 64 MiB of HBM per device.

v0:
```python
import math

import jax
import jax.numpy as jnp
from jax import lax
from jax.sharding import PartitionSpec as P

D = 4096
HEAD_DIM = 64


epsilon = 1e-06


def joined(value, axis, join):
    pieces = jax.tree.map(lambda part: lax.all_gather(part, axis), value)
    head = jax.tree.map(lambda part: part[0], pieces)
    tail = jax.tree.map(lambda part: part[1:], pieces)
    running, _ = lax.scan(lambda running, share: (join(running, share), None), head, tail)
    return running


def position_sums(values):
    return lax.psum(values, "kv")


def combine_parts(former, latter):
    highest = jnp.maximum(former[0], latter[0])
    former_scale = jnp.exp(former[0] - highest)
    latter_scale = jnp.exp(latter[0] - highest)
    totals = former[1] * former_scale + latter[1] * latter_scale
    weighted = former[2] * former_scale[..., None] + latter[2] * latter_scale[..., None]
    return (highest, totals, weighted)


def row_projection(scaled, weight):
    return lax.dot_general(
        scaled, weight, (((1,), (1,)), ((), ())), preferred_element_type=jnp.float32
    )


def square_relu(upward, squares):
    mixer_scale = lax.rsqrt(squares / D + epsilon)[:, None]
    return jnp.square(jax.nn.relu(mixer_scale * upward)).astype(jnp.bfloat16)


def per_device(
    tokens,
    attn_gain,
    query_weight,
    key_weight,
    value_weight,
    forget_weight,
    forget_bias,
    cache_keys,
    cache_values,
    gate_sums,
    output_weight,
    mixer_gain,
    up_weight,
    down_weight,
):
    batch_rows = tokens.shape[0]
    own_width = tokens.shape[1]
    key_heads = cache_keys.shape[1]
    local_heads = gate_sums.shape[1]
    head_group = local_heads // key_heads
    inverse_root = 1.0 / math.sqrt(HEAD_DIM)
    row_block = lax.all_gather(tokens, "tp", axis=1, tiled=True)
    wide_block = row_block.astype(jnp.float32)
    squares = jnp.sum(wide_block * wide_block, axis=1)
    scaled = (wide_block * attn_gain.astype(jnp.float32)).astype(jnp.bfloat16)
    part_query = jnp.dot(scaled, query_weight, preferred_element_type=jnp.float32)
    part_key = row_projection(scaled, key_weight)
    part_value = row_projection(scaled, value_weight)
    part_gate = row_projection(scaled, forget_weight)
    squares = position_sums(squares)
    part_query, part_key, part_value, part_gate = position_sums(
        (part_query, part_key, part_value, part_gate)
    )
    row_scale = lax.rsqrt(squares / D + epsilon)[:, None]
    query_vectors = (
        (row_scale * part_query)
        .astype(jnp.bfloat16)
        .reshape(batch_rows, key_heads, head_group, HEAD_DIM)
    )
    fresh_key_rows = (
        (row_scale * part_key).astype(jnp.bfloat16).reshape(batch_rows, key_heads, HEAD_DIM)
    )
    new_values = (
        (row_scale * part_value).astype(jnp.bfloat16).reshape(batch_rows, key_heads, 1, HEAD_DIM)
    )
    gate_input = lax.dynamic_slice_in_dim(
        row_scale * part_gate + forget_bias[None, :],
        lax.axis_index("tp") * local_heads,
        local_heads,
        1,
    )
    new_gates = jax.nn.log_sigmoid(gate_input).reshape(batch_rows, key_heads, head_group)
    scores = (
        jnp.einsum("bkgd,bkdp->bkgp", query_vectors, cache_keys, preferred_element_type=jnp.float32)
        * inverse_root
    )
    scores = (
        scores + gate_sums.reshape(batch_rows, key_heads, head_group, -1) + new_gates[..., None]
    )
    own_score = (
        jnp.einsum(
            "jwcs,jws->jwc", query_vectors, fresh_key_rows, preferred_element_type=jnp.float32
        )
        * inverse_root
    )
    is_last = lax.axis_index("kv") == lax.axis_size("kv") - 1
    own_score = jnp.where(is_last, own_score, -jnp.inf)
    highest = jnp.maximum(jnp.max(scores, axis=3), own_score)
    weights = jnp.exp(scores - highest[..., None])
    own_weight = jnp.exp(own_score - highest)
    totals = jnp.sum(weights, axis=3) + own_weight
    weighted = jnp.einsum(
        "bkgp,bkdp->bkgd",
        weights,
        cache_values.astype(jnp.float32),
        precision=lax.Precision.HIGHEST,
    )
    weighted = weighted + own_weight[..., None] * new_values.astype(jnp.float32)
    highest, totals, weighted = joined((highest, totals, weighted), "kv", combine_parts)
    attended = (
        (weighted / totals[..., None])
        .astype(jnp.bfloat16)
        .reshape(batch_rows, local_heads * HEAD_DIM)
    )
    attn_part = jnp.dot(attended, output_weight, preferred_element_type=jnp.float32)
    attn_out = lax.psum(attn_part, "tp")
    hidden = (wide_block + attn_out).astype(jnp.bfloat16)
    wide_hidden = hidden.astype(jnp.float32)
    squares_mixer = jnp.sum(wide_hidden * wide_hidden, axis=1)
    scaled_mixer = (wide_hidden * mixer_gain.astype(jnp.float32)).astype(jnp.bfloat16)
    part_up = jnp.dot(scaled_mixer, up_weight, preferred_element_type=jnp.float32)
    squares_mixer = position_sums(squares_mixer)
    up_share = lax.psum_scatter(part_up, "kv", scatter_dimension=1, tiled=True)
    active_share = square_relu(up_share, squares_mixer)
    active = lax.all_gather(active_share, "kv", axis=1, tiled=True)
    down_part = jnp.dot(active, down_weight, preferred_element_type=jnp.float32)
    down_share = lax.psum_scatter(down_part, "tp", scatter_dimension=1, tiled=True)
    own_hidden = lax.dynamic_slice_in_dim(hidden, lax.axis_index("tp") * own_width, own_width, 1)
    return (own_hidden.astype(jnp.float32) + down_share).astype(jnp.bfloat16)


def solution(mesh):
    placed = (
        P("grp", ("kv", "tp")),
        P("kv"),
        P("kv", "tp"),
        P("tp", "kv"),
        P("tp", "kv"),
        P(None, "kv"),
        P(),
        P("grp", "tp", None, "kv"),
        P("grp", "tp", None, "kv"),
        P("grp", "tp", "kv"),
        P("tp", "kv"),
        P("kv"),
        P("kv", "tp"),
        P("tp", "kv"),
    )
    return jax.shard_map(
        per_device, mesh=mesh, in_specs=placed, out_specs=P("grp", ("kv", "tp")), check_vma=False
    )
```

profile of v0, /device:TPU:0, one launch (start us, length us, event | category | flops | bytes accessed | tf_op | source)
XLA Modules:
  0.0 202.3 jit_solution(8363378954103605165)
XLA Ops:
  6.5 0.0 copy-start
  6.5 0.0 all-reduce.3.cloned.1.call-start
  6.5 6.6 %all_gather.24 = bf16[12,1024]{1,0:T(8,128)(2,1)S(1)} all-gather(bf16[12,256]{1,0:T(8,128)(2,1)} %param.16), channel_id=1, replica_groups=mesh['grp'=2,'kv'=4,'tp'=4] {'tp'}, dimensions={1}, use_global_device_ids=true | all-gather | bytes 30720 | tf_op jit(solution)/shard_map/all_gather | solution.py:69
  13.1 0.7 convert_element_type.55
  13.8 0.6 fusion.9
  14.4 0.0 copy-done
  14.4 1.0 fusion.22
  15.4 1.9 fusion.16
  17.3 1.9 fusion.18
  19.2 1.7 fusion.20
  20.9 0.0 all-reduce.3.cloned.1.call-update
  20.9 0.0 reduce-scatter.3.cloned.1.call-start
  21.0 1.4 reshape.34
  22.3 0.7 convert_element_type.66
  23.0 0.7 dynamic-slice
  23.8 33.8 %all-reduce.3.cloned.1.call-done = (f32[12,1024]{1,0:T(8,128)}, f32[12]{0:T(128)}, f32[12,64]{1,0:T(8,128)}, f32[12,256]{1,0:T(8,128)}, f32[12,256]{1,0:T(8,128)}) async-done(((f32[12,1024]{1,0:T(8,128)}, f32[12]{0:T(128)}, f32[12,64]{1,0:T(8,128)}, f32[12,256]{1,0:T(8,128)}, f32[12,256]{1,0:T(8,128)}), (f32[12,1024]{1,0:T(8,128)}, f32[12]{0:T(128)}, f32[12,64]{1,0:T(8,128)}, f32[12,256]{1,0:T(8,128)}, ...) | async-done | bytes 76864 | tf_op jit(solution)/shard_map/psum | solution.py:24
  57.5 0.6 add_rsqrt_fusion.1
  58.2 0.8 fusion.25
  58.9 0.1 copy.31
  59.0 0.1 copy.32
  59.1 0.9 multiply_convert_fusion.1
  60.1 0.1 reshape.33
  60.2 0.8 fusion.24
  61.0 0.1 reshape.53
  61.1 0.2 fusion.32
  61.2 3.8 %fusion.31 = (f32[12,4,4]{2,1,0:T(4,128)S(1)}, f32[12,4,4,1024]{3,2,1,0:T(4,128)S(1)}) fusion(f32[12,4,4]{2,1,0:T(4,128)S(1)} %copy.32, f32[12,4,4,1024]{3,2,1,0:T(4,128)S(1)} %reshape.34, bf16[12,4,4,64]{3,2,1,0:T(4,128)(2,1)S(1)} %reshape.33, bf16[12,4,64,1024]{3,2,1,0:T(8,128)(2,1)} %param.23), kind=kOutput, calls=%fused_computation.49 | convolution fusion | flops 25952064 | bytes 7890432 | tf_op jit(solution)/shard_map/bkgd,bkdp->bkgp/dot_general | solution.py:101
  65.1 0.9 copy-done.1
  65.9 0.4 fusion.5
  66.4 0.1 reshape.37
  66.5 8.1 %convolution_add_fusion = f32[12,4,4,64]{3,2,1,0:T(4,128)S(1)} fusion(bf16[12,4,64,1024]{3,2,1,0:T(8,128)(2,1)} %param.24, f32[12,4,4,1024]{3,2,1,0:T(4,128)} %copy-done.1, f32[12,4,4]{2,1,0:T(4,128)S(1)} %fusion.15, f32[12,4,64]{2,1,0:T(4,128)S(1)} %reshape.37, f32[12,4,4]{2,1,0:T(4,128)S(1)} %get-tuple-element.85), kind=kOutput, calls=%fused_computation.11 | convolution fusion | flops 151216128 | bytes 7140864 | tf_op jit(solution)/shard_map/bkgp,bkdp->bkgd/dot_general | solution.py:119
  74.6 15.2 %all-gather.2 = f32[48,4,4,64]{3,2,1,0:T(4,128)S(1)} all-gather(f32[12,4,4,64]{3,2,1,0:T(4,128)S(1)} %convolution_add_fusion), channel_id=4, replica_groups=mesh['grp'=2,'kv'=4,'tp'=4] {'kv'}, dimensions={0}, use_global_device_ids=true | all-gather | bytes 245760 | tf_op jit(solution)/shard_map/all_gather | solution.py:16
  89.8 13.2 %all-gather.1 = f32[48,4,4]{2,1,0:T(4,128)S(1)} all-gather(f32[12,4,4]{2,1,0:T(4,128)S(1)} %get-tuple-element.84), channel_id=3, replica_groups=mesh['grp'=2,'kv'=4,'tp'=4] {'kv'}, dimensions={0}, use_global_device_ids=true | all-gather | bytes 3840 | tf_op jit(solution)/shard_map/all_gather | solution.py:16
  103.1 13.2 %all-gather = f32[48,4,4]{2,1,0:T(4,128)S(1)} all-gather(f32[12,4,4]{2,1,0:T(4,128)S(1)} %fusion.15), channel_id=2, replica_groups=mesh['grp'=2,'kv'=4,'tp'=4] {'kv'}, dimensions={0}, use_global_device_ids=true | all-gather | bytes 3840 | tf_op jit(solution)/shard_map/all_gather | solution.py:16
  116.3 0.2 copy.38
  116.5 0.1 copy.36
  116.6 0.2 copy.37
  116.8 0.1 copy.35
  116.9 1.8 while.14
  116.9 0.1 copy.48
  117.0 0.1 copy.49
  117.1 0.3 fusion.52
  117.5 0.1 copy.48
  117.6 0.1 copy.49
  117.7 0.3 fusion.52
  118.1 0.1 copy.48
  118.2 0.1 copy.49
  118.3 0.3 fusion.52
  118.7 0.1 copy.39
  118.8 0.1 divide_convert_fusion
  118.9 0.1 reshape.36
  119.0 2.0 fusion.33
  121.0 10.7 %psum.54 = f32[12,1024]{1,0:T(8,128)S(1)} all-reduce(f32[12,1024]{1,0:T(8,128)S(1)} %fusion.33), channel_id=1, replica_groups=mesh['grp'=2,'kv'=4,'tp'=4] {'tp'}, use_global_device_ids=true, to_apply=%region_10.11 | all-reduce | flops 12288 | bytes 98304 | tf_op jit(solution)/shard_map/psum | solution.py:133
  131.7 0.1 fusion.7
  131.8 5.3 %fusion.12 = f32[12,4096]{1,0:T(8,128)} fusion(bf16[1024,4096]{1,0:T(8,128)(2,1)} %param.28, bf16[12,1024]{1,0:T(8,128)(2,1)S(1)} %get-tuple-element.83, f32[1024]{0:T(1024)S(1)} %convert_element_type.66), kind=kOutput, calls=%fused_computation.28 | convolution fusion | flops 100700160 | bytes 8613888 | tf_op jit(solution)/shard_map/dot_general | solution.py:138
  137.1 0.0 reduce-scatter.3.cloned.1.call-update
  137.1 0.0 reduce-scatter.5.cloned.1.call-start
  137.2 10.4 %psum.55 = f32[12]{0:T(128)S(1)} all-reduce(f32[12]{0:T(128)S(1)} %get-tuple-element.82), channel_id=1, replica_groups=mesh['grp'=2,'kv'=4,'tp'=4] {'kv'}, use_global_device_ids=true, to_apply=%region_12.13 | all-reduce | flops 12 | bytes 96 | tf_op jit(solution)/shard_map/psum | solution.py:24
  147.5 9.5 %reduce-scatter.3.cloned.1.call-done = f32[12,1024]{1,0:T(8,128)} async-done(((f32[12,4096]{1,0:T(8,128)}), f32[12,1024]{1,0:T(8,128)}) %reduce-scatter.3.cloned.1.call-update) | async-done | bytes 49168 | tf_op jit(solution)/shard_map/reduce_scatter | solution.py:140
  157.0 0.9 multiply_convert_fusion
  157.9 13.4 %all_gather.31 = bf16[12,4096]{1,0:T(8,128)(2,1)S(1)} all-gather(bf16[12,1024]{1,0:T(8,128)(2,1)S(1)} %multiply_convert_fusion), channel_id=1, replica_groups=mesh['grp'=2,'kv'=4,'tp'=4] {'kv'}, dimensions={1}, use_global_device_ids=true | all-gather | bytes 122880 | tf_op jit(solution)/shard_map/all_gather | solution.py:142
  171.3 5.2 %fusion.34 = f32[12,1024]{1,0:T(8,128)} fusion(bf16[12,4096]{1,0:T(8,128)(2,1)S(1)} %all_gather.31, bf16[4096,1024]{1,0:T(8,128)(2,1)} %param.29), kind=kOutput, calls=%fused_computation.52 | convolution fusion | flops 100663296 | bytes 8536064 | tf_op jit(solution)/shard_map/dot_general | solution.py:143
  176.5 0.0 reduce-scatter.5.cloned.1.call-update
  176.5 18.0 %reduce-scatter.5.cloned.1.call-done = f32[12,256]{1,0:T(8,128)} async-done(((f32[12,1024]{1,0:T(8,128)}), f32[12,256]{1,0:T(8,128)}) %reduce-scatter.5.cloned.1.call-update) | async-done | bytes 12304 | tf_op jit(solution)/shard_map/reduce_scatter | solution.py:144
  194.5 1.3 add_convert_fusion
  (13 shorter events, 0.2 us)
Async XLA Ops:
  6.5 7.9 %copy-start = (bf16[1024,1024]{1,0:T(8,128)(2,1)S(1)}, bf16[1024,1024]{1,0:T(8,128)(2,1)}, u32[]{:S(2)}) copy-start(bf16[1024,1024]{1,0:T(8,128)(2,1)} %param.18) | copy-start | bytes 6291460
  6.5 51.0 %all-reduce.3.cloned.1.call-start = ((), (), s32[]{:S(2)}) async-start(), calls=%async_computation.4 | async-start | bytes 214016 | tf_op jit(solution)/shard_map/psum | solution.py:24
  20.9 136.1 %reduce-scatter.3.cloned.1.call-start = ((), (), s32[]{:S(2)}) async-start(), calls=%async_computation.2 | async-start | bytes 327680 | tf_op jit(solution)/shard_map/reduce_scatter | solution.py:140
  65.1 0.9 copy-start.1
  137.1 57.4 %reduce-scatter.5.cloned.1.call-start = ((), (), s32[]{:S(2)}) async-start(), calls=%async_computation.3 | async-start | bytes 81920 | tf_op jit(solution)/shard_map/reduce_scatter | solution.py:144
Sparse Core Ops, SparseCore 0:
  21.0 36.4 all-reduce.2
  137.2 19.7 reduce-scatter.2
  176.6 17.8 reduce-scatter.4
where the time goes:
time: 203 us; the launch traced here: 202 us
  blocking collectives  82.7 us (41%)
  waiting for transfers between devices  61.3 us (30%)
  matrix products  31 us (15%)
  between operations  13.2 us (7%)
  other arithmetic  9.18 us (5%)
  local copies, waits for them, and re-layouts  4.9 us (2%)
    all_gather x3, blocking collectives, joined(): pieces = jax.tree.map(lambda part: lax.all_gather(part, axis), value)  41.7 us
    psum x1, waiting for transfers between devices, position_sums(): return lax.psum(values, 'kv')  33.8 us
    reduce_scatter x1, waiting for transfers between devices, per_device(): lax.psum_scatter(down_part, 'tp', scatter_dimension=1, tiled=True)  18 us
    all_gather x1, blocking collectives, per_device(): active = lax.all_gather(active_share, 'kv', axis=1, tiled=True)  13.4 us
    psum x1, blocking collectives, per_device(): attn_out = lax.psum(attn_part, 'tp')  10.7 us
    psum x1, blocking collectives, position_sums(): return lax.psum(values, 'kv')  10.4 us
    reduce_scatter x1, waiting for transfers between devices, per_device(): up_share = lax.psum_scatter(part_up, 'kv', scatter_dimension=1, tiled=True)  9.49 us
    dot_general x1, matrix products, per_device(): jnp.einsum('bkgp,bkdp->bkgd', weights, cache_values.astype(jnp.float32),...  8.08 us
  transfers between devices with their start and end apart: 3, of which 3 were waited for; matrix products, arithmetic and copies ran while one was open for 1% of the time, Pallas kernels for 0%

commit v1 on v0

--- a/solution.py
+++ b/solution.py
@@ -1,8 +1,11 @@
+import functools
 import math
 
 import jax
 import jax.numpy as jnp
 from jax import lax
+from jax.experimental import pallas as pl
+from jax.experimental.pallas import tpu as pltpu
 from jax.sharding import PartitionSpec as P
 
 D = 4096
@@ -146,7 +149,436 @@
     return (own_hidden.astype(jnp.float32) + down_share).astype(jnp.bfloat16)
 
 
+F32 = jnp.float32
+BF16 = jnp.bfloat16
+
+
+def nt_dot(left, right):
+    return lax.dot_general(left, right, (((1,), (1,)), ((), ())), preferred_element_type=F32)
+
+
+def nn_dot(left, right):
+    return jnp.dot(left, right, preferred_element_type=F32)
+
+
+def iota(shape, dim):
+    return lax.broadcasted_iota(jnp.int32, shape, dim)
+
+
+def layer_kernel(
+    n_kv,
+    n_tp,
+    width,
+    tok_ref,
+    again_ref,
+    mgain_ref,
+    bias_ref,
+    wq_hbm,
+    wk_hbm,
+    wv_hbm,
+    wf_hbm,
+    ck_hbm,
+    cv_hbm,
+    gs_hbm,
+    wo_hbm,
+    up_hbm,
+    down_hbm,
+    out_ref,
+    wq,
+    wk,
+    wv,
+    wf,
+    ck,
+    cv,
+    gs,
+    wo,
+    up,
+    down,
+    local_sem,
+    up_sem,
+    down_sem,
+    tokb,
+    proj_out,
+    proj_in,
+    small_out,
+    small_in,
+    part_out,
+    part_in,
+    lse_out,
+    lse_in,
+    attn_out,
+    attn_in,
+    sq_out,
+    sq_in,
+    up_out,
+    up_in,
+    act,
+    dn_out,
+    dn_in,
+    hid,
+    fold,
+    ob,
+    send_kv,
+    recv_kv,
+    send_tp,
+    recv_tp,
+):
+    kv = lax.axis_index("kv")
+    tp = lax.axis_index("tp")
+    rows, own = tok_ref.shape
+    block = own * n_tp
+    inner = wq.shape[1]
+    key_width = wk.shape[0]
+    heads = gs.shape[1]
+    dim = inner // heads
+    key_heads = key_width // dim
+    group = heads // key_heads
+    all_heads = wf.shape[0]
+    unit = up.shape[2]
+    inverse_root = 1.0 / math.sqrt(dim)
+
+    sources = (
+        (wq_hbm, wq),
+        (wk_hbm, wk),
+        (wv_hbm, wv),
+        (wf_hbm, wf),
+        (ck_hbm, ck),
+        (gs_hbm, gs),
+        (cv_hbm, cv),
+        (wo_hbm, wo),
+    )
+    loads = []
+    for i, (hbm, vmem) in enumerate(sources):
+        loads.append(pltpu.make_async_copy(hbm, vmem, local_sem.at[i]))
+    up_loads = []
+    down_loads = []
+    for off in range(n_kv):
+        target = lax.rem(kv + off, n_kv)
+        up_loads.append(
+            pltpu.make_async_copy(
+                up_hbm.at[:, pl.ds(pl.multiple_of(target * unit, unit), unit)],
+                up.at[off],
+                up_sem.at[off],
+            )
+        )
+        origin = lax.rem(kv - off + n_kv, n_kv)
+        down_loads.append(
+            pltpu.make_async_copy(
+                down_hbm.at[pl.ds(pl.multiple_of(origin * unit, unit), unit), :],
+                down.at[off],
+                down_sem.at[off],
+            )
+        )
+    own_tok = pltpu.make_async_copy(tok_ref, tokb.at[tp], local_sem.at[len(sources)])
+    own_tok.start()
+    for load in loads:
+        load.start()
+    for off in list(range(1, n_kv)) + [0]:
+        up_loads[off].start()
+    for off in range(n_kv):
+        down_loads[off].start()
+
+    barrier = pltpu.get_barrier_semaphore()
+    for off in range(1, n_tp):
+        pl.semaphore_signal(
+            barrier,
+            inc=1,
+            device_id={"tp": lax.rem(tp + off, n_tp)},
+            device_id_type=pl.DeviceIdType.MESH,
+        )
+    for off in range(1, n_kv):
+        pl.semaphore_signal(
+            barrier,
+            inc=1,
+            device_id={"kv": lax.rem(kv + off, n_kv)},
+            device_id_type=pl.DeviceIdType.MESH,
+        )
+    pl.semaphore_wait(barrier, n_tp + n_kv - 2)
+
+    sent = []
+
+    def send(axis, phase, off, source, target):
+        me, n = (kv, n_kv) if axis == "kv" else (tp, n_tp)
+        sends, recvs = (send_kv, recv_kv) if axis == "kv" else (send_tp, recv_tp)
+        copy = pltpu.make_async_remote_copy(
+            src_ref=source,
+            dst_ref=target,
+            send_sem=sends.at[phase, off],
+            recv_sem=recvs.at[phase, off],
+            device_id={axis: lax.rem(me + off, n)},
+            device_id_type=pl.DeviceIdType.MESH,
+        )
+        copy.start()
+        sent.append(copy)
+        return copy
+
+    tok_copies = [send("tp", 0, off, tok_ref, tokb.at[tp]) for off in range(1, n_tp)]
+
+    lane = iota((heads, inner), 1)
+    spread = (lane // dim) == iota((heads, inner), 0)
+    fold_row, fold_lane = iota((inner, key_width), 0), iota((inner, key_width), 1)
+    fold[...] = jnp.where(
+        (fold_row // (dim * group) == fold_lane // dim) & (fold_row % dim == fold_lane % dim),
+        1.0,
+        0.0,
+    ).astype(BF16)
+    head_of = jnp.where(iota((128, inner), 1) // dim == iota((128, inner), 0), 1.0, 0.0).astype(BF16)
+    lse_out[...] = jnp.zeros_like(lse_out)
+    key_mask = (iota((heads, key_width), 1) // dim) == (iota((heads, key_width), 0) // group)
+    slim_lane = iota((heads, 128), 1)
+    slim_row = iota((heads, 128), 0)
+
+    own_tok.wait()
+    for copy in tok_copies:
+        copy.wait_recv()
+    wide = jnp.concatenate([tokb[j].astype(F32) for j in range(n_tp)], axis=1)
+    squares = jnp.sum(wide * wide, axis=1, keepdims=True)
+    scaled = (wide * again_ref[...].astype(F32)).astype(BF16)
+    for load in loads[:4]:
+        load.wait()
+    part_qkv = jnp.concatenate(
+        [nn_dot(scaled, wq[...]), nt_dot(scaled, wk[...]), nt_dot(scaled, wv[...])], axis=1
+    )
+    proj_out[0:rows, :] = part_qkv.astype(BF16)
+    part_gate = jnp.concatenate(
+        [
+            nt_dot(scaled, wf[...]),
+            jnp.broadcast_to(squares, (rows, small_out.shape[1] - all_heads)),
+        ],
+        axis=1,
+    )
+    small_out[0:rows, :] = part_gate
+    proj_copies = []
+    for off in range(1, n_kv):
+        proj_copies.append(send("kv", 0, off, proj_out, proj_in.at[off]))
+        proj_copies.append(send("kv", 1, off, small_out, small_in.at[off]))
+    for copy in proj_copies:
+        copy.wait_recv()
+    for off in range(1, n_kv):
+        part_qkv = part_qkv + proj_in[off, 0:rows, :].astype(F32)
+        part_gate = part_gate + small_in[off, 0:rows, :]
+    row_scale = lax.rsqrt(part_gate[:, all_heads : all_heads + 1] / width + epsilon)
+    qkv = row_scale * part_qkv
+    queries = qkv[:, :inner].astype(BF16).astype(F32)
+    new_keys = qkv[:, inner : inner + key_width].astype(BF16).astype(F32)
+    new_values = qkv[:, inner + key_width :].astype(BF16).astype(F32)
+    gate_in = row_scale * part_gate + bias_ref[...]
+    gates = jnp.minimum(gate_in, 0.0) - jnp.log1p(jnp.exp(-jnp.abs(gate_in)))
+    folded = []
+    diagonal = jnp.concatenate(
+        [
+            jnp.where(spread, jnp.broadcast_to(queries[b : b + 1, :], (heads, inner)), 0.0).astype(BF16)
+            for b in range(rows)
+        ],
+        axis=0,
+    )
+    folded = nn_dot(diagonal, fold[...])
+    is_last = iota((heads, 1), 0) * 0 + kv == n_kv - 1
+    for load in loads[4:7]:
+        load.wait()
+    for b in range(rows):
+        query = folded[b * heads : (b + 1) * heads, :]
+        gate = jnp.sum(
+            jnp.where(slim_lane == slim_row + tp * heads, gates[b : b + 1, :], 0.0),
+            axis=1,
+            keepdims=True,
+        )
+        scores = nn_dot(query.astype(BF16), ck[b]) * inverse_root + gs[b] + gate
+        own_score = (
+            jnp.sum(query * new_keys[b : b + 1, :], axis=1, keepdims=True) * inverse_root
+        )
+        own_score = jnp.where(is_last, own_score, -jnp.inf)
+        highest = jnp.maximum(jnp.max(scores, axis=1, keepdims=True), own_score)
+        weights = jnp.exp(scores - highest)
+        own_weight = jnp.exp(own_score - highest)
+        totals = jnp.sum(weights, axis=1, keepdims=True) + own_weight
+        weighted = nt_dot(weights.astype(BF16), cv[b]) + own_weight * new_values[b : b + 1, :]
+        ob[b * heads : (b + 1) * heads, :] = jnp.where(key_mask, weighted / totals, 0.0).astype(BF16)
+        lse = highest + jnp.log(totals)
+        lse_out[b : b + 1, :] = jnp.sum(
+            jnp.where(slim_lane == slim_row, lse, 0.0), axis=0, keepdims=True
+        )
+    lse_copies = [send("kv", 2, off, lse_out, lse_in.at[off]) for off in range(1, n_kv)]
+    unfolded = nt_dot(ob[...], fold[...])
+    part = jnp.concatenate(
+        [
+            jnp.sum(
+                jnp.where(spread, unfolded[b * heads : (b + 1) * heads, :], 0.0),
+                axis=0,
+                keepdims=True,
+            )
+            for b in range(rows)
+        ],
+        axis=0,
+    )
+    part_out[0:rows, :] = part.astype(BF16)
+    lse_copies += [send("kv", 3, off, part_out, part_in.at[off]) for off in range(1, n_kv)]
+    for copy in lse_copies:
+        copy.wait_recv()
+    logs = [lse_out[...]] + [lse_in[off] for off in range(1, n_kv)]
+    top = functools.reduce(jnp.maximum, logs)
+    shares = [jnp.exp(log - top) for log in logs]
+    whole = functools.reduce(jnp.add, shares)
+    pieces = []
+    for share in shares:
+        share = share / whole
+        high = share.astype(BF16).astype(F32)
+        pieces += [high, share - high]
+    expanded = nn_dot(jnp.concatenate(pieces, axis=0).astype(BF16), head_of)
+    padded = lse_out.shape[0]
+    attended = jnp.zeros((rows, inner), F32)
+    for off in range(n_kv):
+        at = 2 * off * padded
+        share = expanded[at : at + rows] + expanded[at + padded : at + padded + rows]
+        block_part = part if off == 0 else part_in[off, 0:rows, :].astype(F32)
+        attended = attended + share * block_part
+    loads[7].wait()
+    attn = nn_dot(attended.astype(BF16), wo[...])
+    attn_out[0:rows, :] = attn.astype(BF16)
+    attn_copies = [send("tp", 1, off, attn_out, attn_in.at[off]) for off in range(1, n_tp)]
+    for copy in attn_copies:
+        copy.wait_recv()
+    for off in range(1, n_tp):
+        attn = attn + attn_in[off, 0:rows, :].astype(F32)
+    hidden = (wide + attn).astype(BF16).astype(F32)
+    squares_mixer = jnp.sum(hidden * hidden, axis=1, keepdims=True)
+    sq_out[0:rows, :] = jnp.broadcast_to(squares_mixer, (rows, sq_out.shape[1]))
+    up_copies = [send("kv", 4, off, sq_out, sq_in.at[off]) for off in range(1, n_kv)]
+    for j in range(n_tp):
+        hid[j, 0:rows, :] = hidden[:, j * own : (j + 1) * own]
+    scaled_mixer = (hidden * mgain_ref[...].astype(F32)).astype(BF16)
+    for off in range(1, n_kv):
+        up_loads[off].wait()
+        up_out[off, 0:rows, :] = nn_dot(scaled_mixer, up[off]).astype(BF16)
+        up_copies.append(send("kv", 5, off, up_out.at[off], up_in.at[off]))
+    up_loads[0].wait()
+    upward = nn_dot(scaled_mixer, up[0])
+    for copy in up_copies:
+        copy.wait_recv()
+    for off in range(1, n_kv):
+        upward = upward + up_in[off, 0:rows, :].astype(F32)
+        squares_mixer = squares_mixer + sq_in[off, 0:rows, 0:1]
+    mixer_scale = lax.rsqrt(squares_mixer / width + epsilon)
+    upward = jnp.maximum(mixer_scale * upward, 0.0)
+    active = (upward * upward).astype(BF16)
+    act[0, 0:rows, :] = active
+    act_copies = [send("kv", 6, off, act.at[0], act.at[off]) for off in range(1, n_kv)]
+    down_loads[0].wait()
+    mixed = nn_dot(active, down[0])
+    for off in range(1, n_kv):
+        down_loads[off].wait()
+        act_copies[off - 1].wait_recv()
+        mixed = mixed + nn_dot(act[off, 0:rows, :], down[off])
+    for j in range(n_tp):
+        dn_out[j, 0:rows, :] = mixed[:, j * own : (j + 1) * own].astype(BF16)
+        hid[j, 0:rows, :] = hid[j, 0:rows, :] + mixed[:, j * own : (j + 1) * own]
+    dn_copies = []
+    for off in range(1, n_tp):
+        target = lax.rem(tp + off, n_tp)
+        dn_copies.append(send("tp", 2, off, dn_out.at[target], dn_in.at[off]))
+    result = hid[tp, 0:rows, :]
+    for copy in dn_copies:
+        copy.wait_recv()
+    for off in range(1, n_tp):
+        result = result + dn_in[off, 0:rows, :].astype(F32)
+    out_ref[...] = result.astype(BF16)
+    for copy in sent:
+        copy.wait_send()
+
+
+def fused_device(n_kv, n_tp, *arrays):
+    (tokens, attn_gain, wq, wk, wv, wf, bias, ck, cv, gs, wo, mixer_gain, up, down) = arrays
+    rows, own = tokens.shape
+    batch, key_heads, dim, positions = ck.shape
+    flat = (batch, key_heads * dim, positions)
+    unit = up.shape[1] // n_kv
+    inner = wq.shape[1]
+    key_width = wk.shape[0]
+    heads = gs.shape[1]
+    block = wq.shape[0]
+    padded = -(-rows // 16) * 16
+    slim = -(-(wf.shape[0] + 1) // 128) * 128
+    bias_row = jnp.pad(bias[None, :], ((0, 0), (0, slim - bias.shape[0])))
+    vmem = pltpu.VMEM
+    scratch = [
+        vmem(wq.shape, BF16),
+        vmem(wk.shape, BF16),
+        vmem(wv.shape, BF16),
+        vmem(wf.shape, BF16),
+        vmem(flat, BF16),
+        vmem(flat, BF16),
+        vmem(gs.shape, F32),
+        vmem(wo.shape, BF16),
+        vmem((n_kv, up.shape[0], unit), BF16),
+        vmem((n_kv, unit, down.shape[1]), BF16),
+        pltpu.SemaphoreType.DMA((9,)),
+        pltpu.SemaphoreType.DMA((n_kv,)),
+        pltpu.SemaphoreType.DMA((n_kv,)),
+        vmem((n_tp, rows, own), BF16),
+        vmem((padded, inner + 2 * key_width), BF16),
+        vmem((n_kv, padded, inner + 2 * key_width), BF16),
+        vmem((padded, slim), F32),
+        vmem((n_kv, padded, slim), F32),
+        vmem((padded, inner), BF16),
+        vmem((n_kv, padded, inner), BF16),
+        vmem((padded, 128), F32),
+        vmem((n_kv, padded, 128), F32),
+        vmem((padded, block), BF16),
+        vmem((n_tp, padded, block), BF16),
+        vmem((padded, 128), F32),
+        vmem((n_kv, padded, 128), F32),
+        vmem((n_kv, padded, unit), BF16),
+        vmem((n_kv, padded, unit), BF16),
+        vmem((n_kv, padded, unit), BF16),
+        vmem((n_tp, padded, own), BF16),
+        vmem((n_tp, padded, own), BF16),
+        vmem((n_tp, padded, own), F32),
+        vmem((inner, key_width), BF16),
+        vmem((rows * heads, key_width), BF16),
+        pltpu.SemaphoreType.DMA((7, n_kv)),
+        pltpu.SemaphoreType.DMA((7, n_kv)),
+        pltpu.SemaphoreType.DMA((3, n_tp)),
+        pltpu.SemaphoreType.DMA((3, n_tp)),
+    ]
+    in_vmem = pl.BlockSpec(memory_space=pltpu.VMEM)
+    in_hbm = pl.BlockSpec(memory_space=pl.ANY)
+    return pl.pallas_call(
+        functools.partial(layer_kernel, n_kv, n_tp, D),
+        out_shape=jax.ShapeDtypeStruct((rows, own), BF16),
+        in_specs=[in_vmem] * 4 + [in_hbm] * 10,
+        out_specs=in_vmem,
+        scratch_shapes=scratch,
+        compiler_params=pltpu.CompilerParams(
+            collective_id=0, has_side_effects=True, vmem_limit_bytes=60 * 1024 * 1024
+        ),
+    )(
+        tokens,
+        attn_gain[None, :],
+        mixer_gain[None, :],
+        bias_row,
+        wq,
+        wk,
+        wv,
+        wf,
+        ck.reshape(flat),
+        cv.reshape(flat),
+        gs,
+        wo,
+        up,
+        down,
+    )
+
+
 def solution(mesh):
+    n_kv, n_tp = mesh.shape["kv"], mesh.shape["tp"]
+
+    def device(*arrays):
+        tokens, wk, up = arrays[0], arrays[3], arrays[12]
+        lanes = (tokens.shape[1], wk.shape[0], up.shape[1] // n_kv)
+        if any(width % 128 for width in lanes):
+            return per_device(*arrays)
+        return fused_device(n_kv, n_tp, *arrays)
+
     placed = (
         P("grp", ("kv", "tp")),
         P("kv"),
@@ -164,5 +596,5 @@
         P("tp", "kv"),
     )
     return jax.shard_map(
-        per_device, mesh=mesh, in_specs=placed, out_specs=P("grp", ("kv", "tp")), check_vma=False
-    )
+        device, mesh=mesh, in_specs=placed, out_specs=P("grp", ("kv", "tp")), check_vma=False
+    )

time: 203 us -> 49.5 us (0.24)
  blocking collectives: 82.7 us -> 0 us
  waiting for transfers between devices: 61.3 us -> 0 us
  Pallas kernels: 0 us -> 44.1 us
  matrix products: 31 us -> 0 us
  between operations: 13.2 us -> 0.01 us
  other arithmetic: 9.18 us -> 0 us
    all_gather x5 -> x0, blocking collectives: 61.6 us -> none  [the longest x3 41.7 us: joined(): pieces = jax.tree.map(lambda part: lax.all_gather(part, axis), value)]
    pallas_call x0 -> x1, Pallas kernels: none -> 44.1 us  [fused_device(): pl.pallas_call(functools.partial(layer_kernel, n_kv, n_tp, D), out_shape=...]
    psum x1 -> x0, waiting for transfers between devices: 33.8 us -> none  [position_sums(): return lax.psum(values, 'kv')]
    dot_general x10 -> x0, matrix products: 31 us -> none  [the longest x1 8.08 us: per_device(): jnp.einsum('bkgp,bkdp->bkgd', weights, cache_values.astype(jnp.float32),...]
    reduce_scatter x2 -> x0, waiting for transfers between devices: 27.5 us -> none  [the longest x1 18 us: per_device(): lax.psum_scatter(down_part, 'tp', scatter_dimension=1, tiled=True)]
    psum x2 -> x0, blocking collectives: 21 us -> none  [the longest x1 10.7 us: per_device(): attn_out = lax.psum(attn_part, 'tp')]
    convert_element_type x7 -> x0, other arithmetic: 5.46 us -> none  [the longest x1 1.32 us: per_device(): return (own_hidden.astype(jnp.float32) + down_share).astype(jnp.bfloat16)]
    broadcast_in_dim x0 -> x2, local copies, waits for them, and re-layouts: none -> 2.55 us  [the longest x1 1.28 us: fused_device(): attn_gain[None, :]]
  transfers between devices with their start and end apart: 3 -> 0, of which waited for: 3 -> 0; matrix products, arithmetic and copies ran while one was open for 1% -> 0% of each run, Pallas kernels for 0% -> 0%
where the time goes in v1:
time: 49.5 us; the launch traced here: 49.2 us
  Pallas kernels  44.1 us (89%)
  local copies, waits for them, and re-layouts  5.04 us (10%)
    pallas_call x1, Pallas kernels, fused_device(): pl.pallas_call(functools.partial(layer_kernel, n_kv, n_tp, D), out_shape=...  44.1 us
    unnamed x1, local copies, waits for them, and re-layouts  1.3 us
    broadcast_in_dim x1, local copies, waits for them, and re-layouts, fused_device(): attn_gain[None, :]  1.28 us
    broadcast_in_dim x1, local copies, waits for them, and re-layouts, fused_device(): mixer_gain[None, :]  1.27 us
    pad x1, local copies, waits for them, and re-layouts, fused_device(): bias_row = jnp.pad(bias[None, :], ((0, 0), (0, slim - bias.shape[0])))  1.2 us

profile of v1, /device:TPU:0, one launch (start us, length us, event | category | flops | bytes accessed | tf_op | source)
XLA Modules:
  0.0 49.2 jit_solution(2193299910569538674)
XLA Ops:
  0.0 1.2 %pad.4.bias_ref = f32[1,128]{1,0:T(1,128)} pad(f32[1,64]{1,0:T(1,128)} %bitcast.5, f32[]{:T(128)} %constant.2.clone.1), padding=0_0x0_64 | pad | bytes 772 | tf_op jit(solution)/shard_map/jit(_pad)/pad | solution.py:501
  1.2 1.3 %broadcast_in_dim.9.again_ref = bf16[1,1024]{1,0:T(2,128)(2,1)} reshape(bf16[1024]{0:T(1024)(128)(2,1)} %param.15) | data formatting | bytes 4096 | tf_op jit(solution)/shard_map/broadcast_in_dim | solution.py:556
  2.5 1.3 %broadcast_in_dim.10.mgain_ref = bf16[1,1024]{1,0:T(2,128)(2,1)} reshape(bf16[1024]{0:T(1024)(128)(2,1)} %param.25) | data formatting | bytes 4096 | tf_op jit(solution)/shard_map/broadcast_in_dim | solution.py:557
  3.7 44.1 %shard_map.136 = bf16[12,256]{1,0:T(8,128)(2,1)} custom-call(bf16[12,256]{1,0:T(8,128)(2,1)} %tok_ref.1, bf16[1,1024]{1,0:T(2,128)(2,1)} %broadcast_in_dim.9.again_ref, bf16[1,1024]{1,0:T(2,128)(2,1)} %broadcast_in_dim.10.mgain_ref, f32[1,128]{1,0:T(1,128)} %pad.4.bias_ref, bf16[1024,1024]{1,0:T(8,128)(2,1)} %wq_hbm.1, bf16[256,1024]{1,0:T(8,128)(2,1)} %wk_hbm.1, ...), custom_call_target="tpu_custom_call" | custom-call | tf_op jit(solution)/shard_map/pallas_call | solution.py:545
  47.9 1.3 %copy.16 = bf16[12,256]{1,0:T(8,128)(2,1)} copy(bf16[12,256]{1,0:T(8,128)(2,1)} %shard_map.136) | data formatting | bytes 12288

commit v2 on v1

--- a/solution.py
+++ b/solution.py
@@ -271,12 +271,8 @@
         )
     own_tok = pltpu.make_async_copy(tok_ref, tokb.at[tp], local_sem.at[len(sources)])
     own_tok.start()
-    for load in loads:
+    for load in loads[:4]:
         load.start()
-    for off in list(range(1, n_kv)) + [0]:
-        up_loads[off].start()
-    for off in range(n_kv):
-        down_loads[off].start()
 
     barrier = pltpu.get_barrier_semaphore()
     for off in range(1, n_tp):
@@ -313,6 +309,9 @@
         return copy
 
     tok_copies = [send("tp", 0, off, tok_ref, tokb.at[tp]) for off in range(1, n_tp)]
+
+    for load in loads[4:]:
+        load.start()
 
     lane = iota((heads, inner), 1)
     spread = (lane // dim) == iota((heads, inner), 0)
@@ -333,7 +332,7 @@
         copy.wait_recv()
     wide = jnp.concatenate([tokb[j].astype(F32) for j in range(n_tp)], axis=1)
     squares = jnp.sum(wide * wide, axis=1, keepdims=True)
-    scaled = (wide * again_ref[...].astype(F32)).astype(BF16)
+    scaled = (wide * again_ref[...].astype(F32).reshape(1, block)).astype(BF16)
     for load in loads[:4]:
         load.wait()
     part_qkv = jnp.concatenate(
@@ -352,6 +351,10 @@
     for off in range(1, n_kv):
         proj_copies.append(send("kv", 0, off, proj_out, proj_in.at[off]))
         proj_copies.append(send("kv", 1, off, small_out, small_in.at[off]))
+    for off in list(range(1, n_kv)) + [0]:
+        up_loads[off].start()
+    for off in range(n_kv):
+        down_loads[off].start()
     for copy in proj_copies:
         copy.wait_recv()
     for off in range(1, n_kv):
@@ -362,7 +365,9 @@
     queries = qkv[:, :inner].astype(BF16).astype(F32)
     new_keys = qkv[:, inner : inner + key_width].astype(BF16).astype(F32)
     new_values = qkv[:, inner + key_width :].astype(BF16).astype(F32)
-    gate_in = row_scale * part_gate + bias_ref[...]
+    bias = bias_ref[...].reshape(1, all_heads)
+    bias = jnp.concatenate([bias, jnp.zeros((1, part_gate.shape[1] - all_heads), F32)], axis=1)
+    gate_in = row_scale * part_gate + bias
     gates = jnp.minimum(gate_in, 0.0) - jnp.log1p(jnp.exp(-jnp.abs(gate_in)))
     folded = []
     diagonal = jnp.concatenate(
@@ -446,7 +451,7 @@
     up_copies = [send("kv", 4, off, sq_out, sq_in.at[off]) for off in range(1, n_kv)]
     for j in range(n_tp):
         hid[j, 0:rows, :] = hidden[:, j * own : (j + 1) * own]
-    scaled_mixer = (hidden * mgain_ref[...].astype(F32)).astype(BF16)
+    scaled_mixer = (hidden * mgain_ref[...].astype(F32).reshape(1, block)).astype(BF16)
     for off in range(1, n_kv):
         up_loads[off].wait()
         up_out[off, 0:rows, :] = nn_dot(scaled_mixer, up[off]).astype(BF16)
@@ -498,7 +503,6 @@
     block = wq.shape[0]
     padded = -(-rows // 16) * 16
     slim = -(-(wf.shape[0] + 1) // 128) * 128
-    bias_row = jnp.pad(bias[None, :], ((0, 0), (0, slim - bias.shape[0])))
     vmem = pltpu.VMEM
     scratch = [
         vmem(wq.shape, BF16),
@@ -553,9 +557,9 @@
         ),
     )(
         tokens,
-        attn_gain[None, :],
-        mixer_gain[None, :],
-        bias_row,
+        attn_gain,
+        mixer_gain,
+        bias,
         wq,
         wk,
         wv,

time: 49.5 us -> 45.6 us (0.921)
  local copies, waits for them, and re-layouts: 5.04 us -> 1.3 us
    broadcast_in_dim x2 -> x0, local copies, waits for them, and re-layouts: 2.55 us -> none  [the longest x1 1.28 us: fused_device(): attn_gain[None, :]]
    pad x1 -> x0, local copies, waits for them, and re-layouts: 1.2 us -> none  [fused_device(): bias_row = jnp.pad(bias[None, :], ((0, 0), (0, slim - bias.shape[0])))]
where the time goes in v2:
time: 45.6 us; the launch traced here: 45.4 us
  Pallas kernels  44.1 us (97%)
  local copies, waits for them, and re-layouts  1.3 us (3%)
    pallas_call x1, Pallas kernels, fused_device(): pl.pallas_call(functools.partial(layer_kernel, n_kv, n_tp, D), out_shape=...  44.1 us
    unnamed x1, local copies, waits for them, and re-layouts  1.3 us

profile of v2, /device:TPU:0, one launch (start us, length us, event | category | flops | bytes accessed | tf_op | source)
XLA Modules:
  0.0 45.4 jit_solution(3180964885384248861)
XLA Ops:
  0.0 44.1 %shard_map.136 = bf16[12,256]{1,0:T(8,128)(2,1)} custom-call(bf16[12,256]{1,0:T(8,128)(2,1)} %tok_ref.1, bf16[1024]{0:T(1024)(128)(2,1)} %again_ref.1, bf16[1024]{0:T(1024)(128)(2,1)} %mgain_ref.1, f32[64]{0:T(128)} %bias_ref.1, bf16[1024,1024]{1,0:T(8,128)(2,1)} %wq_hbm.1, bf16[256,1024]{1,0:T(8,128)(2,1)} %wk_hbm.1, bf16[256,1024]{1,0:T(8,128)(2,1)} %wv_hbm.1, ...), custom_call_target="tpu_custom_call" | custom-call | tf_op jit(solution)/shard_map/pallas_call | solution.py:549
  44.1 1.3 %copy.16 = bf16[12,256]{1,0:T(8,128)(2,1)} copy(bf16[12,256]{1,0:T(8,128)(2,1)} %shard_map.136) | data formatting | bytes 12288
